TPU v7x, 128 devices: a whole 4x4x4 slice. The times are simulated.
128 devices in a mesh: ep: 32 (over z, y, core), tp: 4 (over x).
Axes of the slice: x: 4, y: 4, z: 4, core: 2. Of those that a mesh axis runs over, the one named last changes fastest.
Arguments:
- tokens: bfloat16 [16384, 2048], P(('ep', 'tp')), may hold values from -6 to 6
- norm_gain: float32 [2048], replicated, may hold values from 0.1 to 1.9
- w_gate: bfloat16 [128, 2048, 512], P(('ep', 'tp')), may hold values from -0.125 to 0.125
- w_up: bfloat16 [128, 2048, 512], P(('ep', 'tp')), may hold values from -0.125 to 0.125
- w_down: bfloat16 [128, 512, 2048], P(('ep', 'tp')), may hold values from -0.25 to 0.25
- routing: int32 [16384, 2], P(('ep', 'tp')), may hold values from 0 to 127, as said below
- gate_weight: float32 [16384, 2], P(('ep', 'tp')), may hold values from 0.05 to 1
Outputs:
- combined: bfloat16 [16384, 2048], P(('ep', 'tp'))
Inputs may be any that keep to these rules, and one draw needn't show every extreme that they name: `routing`: A token's 2 experts are distinct and lie in one group of 4 consecutive experts. Of the 128 tokens of each device exactly 4 choose each group; no expert is named by more than 4 tokens of one device, and in every group one expert is named by exactly 4 tokens of every device.
All inputs are finite; a program needn't handle non-finite values.
Results may differ from a plain program's by a relative error of at most 0.0085.
Values may be sent and summed in bfloat16 or wider, within the bound.
No kernel may reach another device: no remote copies, remote signals or barrier semaphores. Data moves between devices by JAX's collectives and lax.ppermute only.
A program may use at most 64 MiB of HBM per device.

v0:
```python
import jax
import jax.numpy as jnp
from jax import lax
from jax.sharding import PartitionSpec as P


def local(tokens, norm_gain, w_gate, w_up, w_down, routing, gate_weight):
    tok_rows, width = tokens.shape
    ep_count = lax.axis_size("ep")
    tp_count = lax.axis_size("tp")
    experts = ep_count * tp_count
    capacity = 4 * tok_rows // experts
    values = tokens.astype(jnp.float32)
    scale = lax.rsqrt(jnp.mean(values * values, axis=-1, keepdims=True) + 1e-06)
    normed = (values * scale * norm_gain).astype(jnp.bfloat16)
    normed_pad = jnp.concatenate([normed, jnp.zeros((1, width), jnp.bfloat16)], axis=0)
    assigned = routing.reshape(-1)
    onehot = (assigned[:, None] == jnp.arange(experts, dtype=jnp.int32)[None, :]).astype(jnp.int32)
    running = jnp.cumsum(onehot, axis=0)
    slot_index = jnp.sum(onehot * running, axis=1) - 1
    position = assigned * capacity + slot_index
    slot_owner = jnp.full((experts * capacity,), tok_rows, jnp.int32)
    slot_owner = slot_owner.at[position].set(
        jnp.arange(assigned.shape[0], dtype=jnp.int32) // routing.shape[1]
    )
    outgoing = normed_pad[slot_owner].reshape(experts, capacity, width)
    arrived = lax.all_to_all(outgoing, ("ep", "tp"), split_axis=0, concat_axis=0, tiled=True)
    slot_rows = arrived.reshape(-1, width)
    gate_part = jnp.dot(slot_rows, w_gate[0], preferred_element_type=jnp.float32)
    up_part = jnp.dot(slot_rows, w_up[0], preferred_element_type=jnp.float32)
    hidden = (jax.nn.silu(gate_part) * up_part).astype(jnp.bfloat16)
    expert_out = jnp.dot(hidden, w_down[0], preferred_element_type=jnp.float32).astype(jnp.bfloat16)
    answered = expert_out.reshape(arrived.shape)
    returned = lax.all_to_all(answered, ("ep", "tp"), split_axis=0, concat_axis=0, tiled=True)
    picked = returned.reshape(experts * capacity, width)[position]
    picked = picked.reshape(tok_rows, routing.shape[1], width).astype(jnp.float32)
    combined = jnp.sum(gate_weight[:, :, None] * picked, axis=1)
    return combined.astype(jnp.bfloat16)


def solution(mesh):
    placed = (
        P(("ep", "tp"), None),
        P(),
        P(("ep", "tp"), None, None),
        P(("ep", "tp"), None, None),
        P(("ep", "tp"), None, None),
        P(("ep", "tp"), None),
        P(("ep", "tp"), None),
    )
    return jax.shard_map(
        local, mesh=mesh, in_specs=placed, out_specs=P(("ep", "tp"), None), check_vma=False
    )
```

profile of v0, /device:TPU:1, one launch (start us, length us, event | category | flops | bytes accessed | tf_op | source)
XLA Modules:
  0.0 126.6 jit_solution(14652439876208420146)
XLA Ops:
  0.0 0.9 copy.11
  0.9 0.1 eq.29
  1.1 0.1 eq.25
  1.2 0.7 broadcast_multiply_fusion
  2.0 0.2 fusion.17
  2.3 0.2 fusion.18
  2.5 0.1 copy.10
  2.6 0.1 mul.61
  2.8 1.4 %scatter_custom_fusion = s32[512]{0:T(512)S(1)} fusion(s32[256]{0:T(256)S(1)} %bitcast.33, s32[256]{0:T(256)S(1)} %and_select_fusion, s32[]{:T(128)} %constant.37.clone.1), kind=kCustom, calls=%fused_computation.35 | custom fusion | bytes 2052 | tf_op jit(solution)/shard_map/scatter | solution.py:23
  4.2 1.2 fusion.11
  5.5 0.9 fusion.13
  6.4 3.3 %gather_fusion = bf16[512,2048]{1,0:T(8,128)(2,1)} fusion(bf16[129,2048]{1,0:T(8,128)(2,1)S(1)} %concatenate.3, s32[1024]{0:T(1024)S(1)} %pad_clamp_fusion.1), kind=kCustom, calls=%fused_computation | custom fusion | bytes 4196352 | tf_op jit(solution)/shard_map/gather | solution.py:26
  9.7 4.1 %reshape.77 = bf16[128,4,2048]{2,1,0:T(4,128)(2,1)} reshape(bf16[512,2048]{1,0:T(8,128)(2,1)} %gather_fusion) | data formatting | bytes 4194304 | tf_op jit(solution)/shard_map/reshape | solution.py:26
  13.8 42.4 %all_to_all.10 = bf16[128,4,2048]{2,1,0:T(4,128)(2,1)} all-to-all(bf16[128,4,2048]{2,1,0:T(4,128)(2,1)} %reshape.77), channel_id=1, replica_groups=mesh['ep'=32,'tp'=4] {'ep','tp'}, dimensions={0} | all-to-all | bytes 4194304 | tf_op jit(solution)/shard_map/all_to_all | solution.py:27
  56.2 4.0 %reshape.78 = bf16[512,2048]{1,0:T(8,128)(2,1)} reshape(bf16[128,4,2048]{2,1,0:T(4,128)(2,1)} %all_to_all.10) | data formatting | bytes 4194304 | tf_op jit(solution)/shard_map/reshape | solution.py:28
  60.1 4.4 %fusion.3 = f32[512,512]{1,0:T(8,128)} fusion(bf16[512,2048]{1,0:T(8,128)(2,1)} %reshape.78, bf16[1,2048,512]{2,1,0:T(8,128)(2,1)} %param.9), kind=kOutput, calls=%fused_computation.7 | convolution fusion | flops 1073741824 | bytes 5242880 | tf_op jit(solution)/shard_map/dot_general | solution.py:29
  64.6 6.2 %convolution_convert_fusion = bf16[512,2048]{1,0:T(8,128)(2,1)} fusion(bf16[1,512,2048]{2,1,0:T(8,128)(2,1)S(1)} %copy-done, bf16[512,2048]{1,0:T(8,128)(2,1)} %reshape.78, bf16[1,2048,512]{2,1,0:T(8,128)(2,1)} %param.10, f32[512,512]{1,0:T(8,128)} %fusion.3), kind=kOutput, calls=%fused_computation.3 | convolution fusion | flops 2150105088 | bytes 9437184 | tf_op jit(solution)/shard_map/dot_general | solution.py:32
  70.8 4.1 %reshape.79 = bf16[128,4,2048]{2,1,0:T(4,128)(2,1)} reshape(bf16[512,2048]{1,0:T(8,128)(2,1)} %convolution_convert_fusion) | data formatting | bytes 4194304 | tf_op jit(solution)/shard_map/reshape | solution.py:33
  74.9 5.0 %all-to-all-start.1 = ((bf16[128,4,2048]{2,1,0:T(4,128)(2,1)}), bf16[128,4,2048]{2,1,0:T(4,128)(2,1)}, u32[]{:S(2)}, u32[]{:S(2)}) async-start(bf16[128,4,2048]{2,1,0:T(4,128)(2,1)} %reshape.79), calls=%async_computation.1 | async-start | bytes 4194304 | tf_op jit(solution)/shard_map/all_to_all | solution.py:34
  80.1 30.4 %all-to-all-done.1 = bf16[128,4,2048]{2,1,0:T(4,128)(2,1)} async-done(((bf16[128,4,2048]{2,1,0:T(4,128)(2,1)}), bf16[128,4,2048]{2,1,0:T(4,128)(2,1)}, u32[]{:S(2)}, u32[]{:S(2)}) %all-to-all-start.1) | async-done | bytes 2097184 | tf_op jit(solution)/shard_map/all_to_all | solution.py:34
  110.4 4.0 %reshape.80 = bf16[512,2048]{1,0:T(8,128)(2,1)} reshape(bf16[128,4,2048]{2,1,0:T(4,128)(2,1)} %all-to-all-done.1) | data formatting | bytes 4194304 | tf_op jit(solution)/shard_map/reshape | solution.py:35
  114.4 4.2 %gather_fusion.1 = bf16[256,2048]{1,0:T(8,128)(2,1)S(1)} fusion(bf16[512,2048]{1,0:T(8,128)(2,1)} %reshape.80, s32[1024]{0:T(1024)S(1)} %pad_clamp_fusion), kind=kCustom, calls=%fused_computation.1 | custom fusion | bytes 2098176 | tf_op jit(solution)/shard_map/gather | solution.py:35
  118.6 2.4 %reshape.81 = f32[128,2,2048]{2,1,0:T(2,128)} reshape(bf16[256,2048]{1,0:T(8,128)(2,1)S(1)} %gather_fusion.1) | data formatting | bytes 3145728 | tf_op jit(solution)/shard_map/convert_element_type | solution.py:36
  121.0 5.6 %multiply_reduce_fusion = bf16[128,2048]{1,0:T(8,128)(2,1)} fusion(f32[128,2,2048]{2,1,0:T(2,128)} %reshape.81, f32[128,2]{1,0:T(8,128)S(1)} %copy.9), kind=kLoop, calls=%fused_computation.9 | loop fusion | flops 786432 | bytes 2622464 | tf_op jit(solution)/shard_map/reduce_sum | solution.py:37
  (22 shorter events, 0.4 us)
Async XLA Ops:
  0.0 64.6 %copy-start = (bf16[1,512,2048]{2,1,0:T(8,128)(2,1)S(1)}, bf16[1,512,2048]{2,1,0:T(8,128)(2,1)}, u32[]{:S(2)}) copy-start(bf16[1,512,2048]{2,1,0:T(8,128)(2,1)} %param.11) | copy-start | bytes 6291460
  0.0 5.5 %copy-start.1 = (bf16[128,2048]{1,0:T(8,128)(2,1)S(1)}, bf16[128,2048]{1,0:T(8,128)(2,1)}, u32[]{:S(2)}) copy-start(bf16[128,2048]{1,0:T(8,128)(2,1)} %param.7) | copy-start | bytes 1572868
  74.9 5.0 %copy-start.2 = (f32[128,2]{0,1:T(2,128)S(1)}, f32[128,2]{0,1:T(2,128)}, u32[]{:S(2)}) copy-start(f32[128,2]{0,1:T(2,128)} %param.13) | copy-start | bytes 3076
  74.9 35.5 %all-to-all-start.1 = ((bf16[128,4,2048]{2,1,0:T(4,128)(2,1)}), bf16[128,4,2048]{2,1,0:T(4,128)(2,1)}, u32[]{:S(2)}, u32[]{:S(2)}) async-start(bf16[128,4,2048]{2,1,0:T(4,128)(2,1)} %reshape.79), calls=%async_computation.1 | async-start | bytes 4194304 | tf_op jit(solution)/shard_map/all_to_all | solution.py:34
where the time goes:
time: 127 us
  blocking collectives  42.4 us (33%)
  waiting for transfers between devices  30.4 us (24%)
  local copies, waits for them, and re-layouts  29.2 us (23%)
  matrix products  10.7 us (8%)
  other arithmetic  8.86 us (7%)
  starting transfers between devices  5.02 us (4%)
    all_to_all x1, blocking collectives, local(): lax.all_to_all(outgoing, ('ep', 'tp'), split_axis=0, concat_axis=0, tiled...  42.4 us
    all_to_all x1, waiting for transfers between devices, local(): lax.all_to_all(answered, ('ep', 'tp'), split_axis=0, concat_axis=0, tiled...  30.4 us
    dot_general x1, matrix products, local(): jnp.dot(hidden, w_down[0], preferred_element_type=jnp.float32)  6.22 us
    reduce_sum x1, other arithmetic, local(): combined = jnp.sum(gate_weight[:, :, None] * picked, axis=1)  5.59 us
    all_to_all x1, starting transfers between devices, local(): lax.all_to_all(answered, ('ep', 'tp'), split_axis=0, concat_axis=0, tiled...  5.02 us
    dot_general x1, matrix products, local(): jnp.dot(slot_rows, w_gate[0], preferred_element_type=jnp.float32)  4.44 us
    gather x1, local copies, waits for them, and re-layouts, local(): picked = returned.reshape(experts * capacity, width)[position]  4.22 us
    reshape x1, local copies, waits for them, and re-layouts, local(): answered = expert_out.reshape(arrived.shape)  4.11 us
  transfers between devices with their start and end apart: 1, of which 1 were waited for; matrix products, arithmetic and copies ran while one was open for 0% of the time, Pallas kernels for 0%

commit v1 on v0

v1 whole, which is shorter than its diff:
```python
import jax
import jax.numpy as jnp
from jax import lax
from jax.experimental import pallas as pl
from jax.experimental.pallas import tpu as pltpu
from jax.sharding import PartitionSpec as P

AXES = ("ep", "tp")
BF = jnp.bfloat16
F32 = jnp.float32


def rank_in_group(group, groups):
    n = group.shape[1]
    member = lax.broadcasted_iota(jnp.int32, (groups, n), 0) == group
    earlier = lax.broadcasted_iota(jnp.int32, (n, n), 0) < lax.broadcasted_iota(jnp.int32, (n, n), 1)
    counts = jnp.dot(member.astype(BF), earlier.astype(BF), preferred_element_type=F32)
    return jnp.sum(jnp.where(member, counts, 0.0), axis=0, keepdims=True).astype(jnp.int32)


def dispatch_kernel(groups, members, tok_ref, gain_ref, route_ref, out_ref):
    rows, width = tok_ref.shape
    slots = rows // groups
    group = route_ref[0:1, :] // members
    place = group * slots + rank_in_group(group, groups)
    pick = (lax.broadcasted_iota(jnp.int32, (rows, rows), 0) == place).astype(BF)
    values = tok_ref[...].astype(F32)
    scale = lax.rsqrt(jnp.mean(values * values, axis=-1, keepdims=True) + 1e-06)
    normed = (values * scale * gain_ref[...]).astype(BF)
    ordered = jnp.dot(pick, normed, preferred_element_type=F32).astype(BF)
    ordered = ordered.reshape(groups, slots, width)
    for m in range(members):
        out_ref[:, m] = ordered


def expert_kernel(x_ref, wg_ref, wu_ref, wd_ref, out_ref):
    blocks, slots, width = x_ref.shape
    step = blocks // 2
    for c in range(2):
        x = x_ref[c * step:(c + 1) * step].reshape(step * slots, width)
        gate = jnp.dot(x, wg_ref[...], preferred_element_type=F32)
        up = jnp.dot(x, wu_ref[...], preferred_element_type=F32)
        hidden = (gate / (1.0 + jnp.exp(-gate)) * up).astype(BF)
        out = jnp.dot(hidden, wd_ref[...], preferred_element_type=F32).astype(BF)
        out_ref[c * step:(c + 1) * step] = out.reshape(step, slots, width)


def combine_kernel(groups, members, r_ref, route_ref, gw_ref, out_ref):
    blocks, slots, width = r_ref.shape
    rows = out_ref.shape[0]
    e0, e1 = route_ref[0:1, :], route_ref[1:2, :]
    rank = rank_in_group(e0 // members, groups)
    row = lax.broadcasted_iota(jnp.int32, (blocks * slots, rows), 0)
    expert = row // slots
    weight = jnp.where(expert == e0, gw_ref[0:1, :], 0.0) + jnp.where(expert == e1, gw_ref[1:2, :], 0.0)
    weight = jnp.where(row % slots == rank, weight, 0.0)
    high = weight.astype(BF)
    low = (weight - high.astype(F32)).astype(BF)
    both = jnp.concatenate([high, low], axis=1)
    r = r_ref[...].reshape(blocks * slots, width)
    out = lax.dot_general(both, r, (((0,), (0,)), ((), ())), preferred_element_type=F32)
    out_ref[...] = (out[:rows] + out[rows:]).astype(BF)


def local(tokens, norm_gain, w_gate, w_up, w_down, routing, gate_weight):
    rows, width = tokens.shape
    groups = lax.axis_size("ep")
    members = lax.axis_size("tp")
    experts = groups * members
    slots = rows // groups
    route = routing.T
    weights = gate_weight.T
    params = pltpu.CompilerParams(vmem_limit_bytes=48 * 1024 * 1024)
    outgoing = pl.pallas_call(
        lambda *refs: dispatch_kernel(groups, members, *refs),
        out_shape=jax.ShapeDtypeStruct((groups, members, slots, width), BF),
        compiler_params=params,
        name="dispatch",
    )(tokens, norm_gain.reshape(1, width), route)
    arrived = lax.all_to_all(outgoing.reshape(experts, slots, width), AXES, split_axis=0, concat_axis=0, tiled=True)
    answered = pl.pallas_call(
        expert_kernel,
        out_shape=jax.ShapeDtypeStruct((experts, slots, width), BF),
        compiler_params=params,
        name="expert",
    )(arrived, w_gate[0], w_up[0], w_down[0])
    returned = lax.all_to_all(answered, AXES, split_axis=0, concat_axis=0, tiled=True)
    return pl.pallas_call(
        lambda *refs: combine_kernel(groups, members, *refs),
        out_shape=jax.ShapeDtypeStruct((rows, width), BF),
        compiler_params=params,
        name="combine",
    )(returned, route, weights)


def solution(mesh):
    placed = (
        P(AXES, None),
        P(),
        P(AXES, None, None),
        P(AXES, None, None),
        P(AXES, None, None),
        P(AXES, None),
        P(AXES, None),
    )
    return jax.shard_map(local, mesh=mesh, in_specs=placed, out_specs=P(AXES, None), check_vma=False)
```

time: 127 us -> 87.7 us (0.69)
  blocking collectives: 42.4 us -> 76.2 us
  waiting for transfers between devices: 30.4 us -> 0 us
  local copies, waits for them, and re-layouts: 29.2 us -> 2.43 us
  matrix products: 10.7 us -> 0 us
  other arithmetic: 8.86 us -> 0 us
  Pallas kernels: 0 us -> 8.76 us
  starting transfers between devices: 5.02 us -> 0 us
    all_to_all x1 -> x2, blocking collectives: 42.4 us -> 76.2 us  [the longest x1 42 us: local(): lax.all_to_all(outgoing.reshape(experts, slots, width), AXES, split_axis=...]
    all_to_all x1 -> x0, waiting for transfers between devices: 30.4 us -> none  [local(): lax.all_to_all(answered, ('ep', 'tp'), split_axis=0, concat_axis=0, tiled...]
    reshape x4 -> x0, local copies, waits for them, and re-layouts: 16.1 us -> none  [the longest x1 4.11 us: local(): answered = expert_out.reshape(arrived.shape)]
    dot_general x2 -> x0, matrix products: 10.7 us -> none  [the longest x1 6.22 us: local(): jnp.dot(hidden, w_down[0], preferred_element_type=jnp.float32)]
    pallas_call x0 -> x3, Pallas kernels: none -> 8.76 us  [the longest x1 6.45 us: local(): pl.pallas_call(expert_kernel, out_shape=jax.ShapeDtypeStruct((experts, sl...]
    gather x2 -> x0, local copies, waits for them, and re-layouts: 7.52 us -> none  [the longest x1 4.22 us: local(): picked = returned.reshape(experts * capacity, width)[position]]
    reduce_sum x3 -> x0, other arithmetic: 6.99 us -> none  [the longest x1 5.59 us: local(): combined = jnp.sum(gate_weight[:, :, None] * picked, axis=1)]
    all_to_all x1 -> x0, starting transfers between devices: 5.02 us -> none  [local(): lax.all_to_all(answered, ('ep', 'tp'), split_axis=0, concat_axis=0, tiled...]
  transfers between devices with their start and end apart: 1 -> 0, of which waited for: 1 -> 0; matrix products, arithmetic and copies ran while one was open for 0% -> 0% of each run, Pallas kernels for 0% -> 0%
where the time goes in v1:
time: 87.7 us; the launch traced here: 87.4 us
  blocking collectives  76.2 us (87%)
  Pallas kernels  8.76 us (10%)
  local copies, waits for them, and re-layouts  2.43 us (3%)
    all_to_all x1, blocking collectives, local(): lax.all_to_all(outgoing.reshape(experts, slots, width), AXES, split_axis=...  42 us
    all_to_all x1, blocking collectives, local(): lax.all_to_all(answered, AXES, split_axis=0, concat_axis=0, tiled=True)  34.2 us
    pallas_call x1, Pallas kernels, local(): pl.pallas_call(expert_kernel, out_shape=jax.ShapeDtypeStruct((experts, sl...  6.45 us
    unnamed x10, local copies, waits for them, and re-layouts  2.43 us

profile of v1, /device:TPU:1, one launch (start us, length us, event | category | flops | bytes accessed | tf_op | source)
XLA Modules:
  0.0 87.4 jit_solution(16477679428194233768)
XLA Ops:
  0.0 0.0 copy-start
  0.0 1.0 %copy-done = bf16[128,2048]{1,0:T(8,128)(2,1)S(1)} copy-done((bf16[128,2048]{1,0:T(8,128)(2,1)S(1)}, bf16[128,2048]{1,0:T(8,128)(2,1)}, u32[]{:S(2)}) %copy-start) | copy-done | bytes 524312
  1.0 0.0 copy-start.1
  1.0 0.7 copy-done.1
  1.7 0.0 copy-start.2
  1.7 0.7 copy-done.2
  2.4 0.6 dispatch.1
  3.0 42.0 %all_to_all.10.x_ref = bf16[128,4,2048]{2,1,0:T(4,128)(2,1)S(1)} all-to-all(bf16[128,4,2048]{2,1,0:T(4,128)(2,1)S(1)} %bitcast.7), channel_id=1, replica_groups=mesh['ep'=32,'tp'=4] {'ep','tp'}, dimensions={0} | all-to-all | bytes 4194304 | tf_op jit(solution)/shard_map/all_to_all | solution.py:80
  45.1 6.5 %expert.1 = bf16[128,4,2048]{2,1,0:T(4,128)(2,1)S(1)} custom-call(bf16[128,4,2048]{2,1,0:T(4,128)(2,1)S(1)} %all_to_all.10.x_ref, bf16[2048,512]{1,0:T(8,128)(2,1)} %bitcast.12, bf16[2048,512]{1,0:T(8,128)(2,1)} %bitcast.13, bf16[512,2048]{1,0:T(8,128)(2,1)} %bitcast.14), custom_call_target="tpu_custom_call" | custom-call | tf_op jit(solution)/shard_map/expert/pallas_call | solution.py:81
  51.5 0.0 copy-start.3
  51.6 0.0 copy-start.4
  51.6 34.2 %all_to_all.11.refs_0_ = bf16[128,4,2048]{2,1,0:T(4,128)(2,1)S(1)} all-to-all(bf16[128,4,2048]{2,1,0:T(4,128)(2,1)S(1)} %expert.1), channel_id=1, replica_groups=mesh['ep'=32,'tp'=4] {'ep','tp'}, dimensions={0} | all-to-all | bytes 4194304 | tf_op jit(solution)/shard_map/all_to_all | solution.py:87
  85.7 0.0 copy-done.3
  85.7 0.0 copy-done.4
  85.7 1.7 %combine.1 = bf16[128,2048]{1,0:T(8,128)(2,1)} custom-call(bf16[128,4,2048]{2,1,0:T(4,128)(2,1)S(1)} %all_to_all.11.refs_0_, s32[2,128]{1,0:T(2,128)S(1)} %bitcast.10, f32[2,128]{1,0:T(2,128)S(1)} %bitcast.11), custom_call_target="tpu_custom_call" | custom-call | tf_op jit(solution)/shard_map/combine/pallas_call | solution.py:88
Async XLA Ops:
  0.0 1.0 %copy-start = (bf16[128,2048]{1,0:T(8,128)(2,1)S(1)}, bf16[128,2048]{1,0:T(8,128)(2,1)}, u32[]{:S(2)}) copy-start(bf16[128,2048]{1,0:T(8,128)(2,1)} %refs_0_.1) | copy-start | bytes 1572868
  1.0 0.7 copy-start.1
  1.7 0.7 copy-start.2
  51.5 34.2 %copy-start.3 = (s32[128,2]{0,1:T(2,128)S(1)}, s32[128,2]{0,1:T(2,128)}, u32[]{:S(2)}) copy-start(s32[128,2]{0,1:T(2,128)} %param.12) | copy-start | bytes 3076
  51.6 34.2 %copy-start.4 = (f32[128,2]{0,1:T(2,128)S(1)}, f32[128,2]{0,1:T(2,128)}, u32[]{:S(2)}) copy-start(f32[128,2]{0,1:T(2,128)} %param.13) | copy-start | bytes 3076

commit v2 on v1

--- a/solution.py
+++ b/solution.py
@@ -36,11 +36,15 @@
 def expert_kernel(x_ref, wg_ref, wu_ref, wd_ref, out_ref):
     blocks, slots, width = x_ref.shape
     step = blocks // 2
+    half = wg_ref.shape[1] // 2
     for c in range(2):
         x = x_ref[c * step:(c + 1) * step].reshape(step * slots, width)
-        gate = jnp.dot(x, wg_ref[...], preferred_element_type=F32)
-        up = jnp.dot(x, wu_ref[...], preferred_element_type=F32)
-        hidden = (gate / (1.0 + jnp.exp(-gate)) * up).astype(BF)
+        parts = []
+        for n in range(2):
+            gate = jnp.dot(x, wg_ref[:, n * half:(n + 1) * half], preferred_element_type=F32)
+            up = jnp.dot(x, wu_ref[:, n * half:(n + 1) * half], preferred_element_type=F32)
+            parts.append((gate / (1.0 + jnp.exp(-gate)) * up).astype(BF))
+        hidden = jnp.concatenate(parts, axis=1)
         out = jnp.dot(hidden, wd_ref[...], preferred_element_type=F32).astype(BF)
         out_ref[c * step:(c + 1) * step] = out.reshape(step, slots, width)
 
@@ -70,7 +74,7 @@
     slots = rows // groups
     route = routing.T
     weights = gate_weight.T
-    params = pltpu.CompilerParams(vmem_limit_bytes=48 * 1024 * 1024)
+    params = pltpu.CompilerParams(vmem_limit_bytes=20 * 1024 * 1024)
     outgoing = pl.pallas_call(
         lambda *refs: dispatch_kernel(groups, members, *refs),
         out_shape=jax.ShapeDtypeStruct((groups, members, slots, width), BF),
@@ -78,8 +82,11 @@
         name="dispatch",
     )(tokens, norm_gain.reshape(1, width), route)
     arrived = lax.all_to_all(outgoing.reshape(experts, slots, width), AXES, split_axis=0, concat_axis=0, tiled=True)
+    in_vmem = pl.BlockSpec(memory_space=pltpu.VMEM)
     answered = pl.pallas_call(
         expert_kernel,
+        in_specs=[in_vmem] * 4,
+        out_specs=in_vmem,
         out_shape=jax.ShapeDtypeStruct((experts, slots, width), BF),
         compiler_params=params,
         name="expert",

time: 87.7 us -> 84.7 us (0.966)
  Pallas kernels: 8.76 us -> 5.73 us
    pallas_call x1, Pallas kernels: 6.45 us -> 3.44 us  [local(): pl.pallas_call(expert_kernel, in_specs=[in_vmem] * 4, out_specs=in_vmem,...]
    unnamed x10 -> x16, local copies, waits for them, and re-layouts: 2.43 us -> 2.44 us
where the time goes in v2:
time: 84.7 us; the launch traced here: 84.4 us
  blocking collectives  76.2 us (90%)
  Pallas kernels  5.73 us (7%)
  local copies, waits for them, and re-layouts  2.44 us (3%)
    all_to_all x1, blocking collectives, local(): lax.all_to_all(outgoing.reshape(experts, slots, width), AXES, split_axis=...  42.1 us
    all_to_all x1, blocking collectives, local(): lax.all_to_all(answered, AXES, split_axis=0, concat_axis=0, tiled=True)  34.2 us
    pallas_call x1, Pallas kernels, local(): pl.pallas_call(expert_kernel, in_specs=[in_vmem] * 4, out_specs=in_vmem,...  3.44 us
    unnamed x16, local copies, waits for them, and re-layouts  2.44 us
    pallas_call x1, Pallas kernels, local(): pl.pallas_call(lambda *refs: combine_kernel(groups, members, *refs), out_...  1.7 us

profile of v2, /device:TPU:1, one launch (start us, length us, event | category | flops | bytes accessed | tf_op | source)
XLA Modules:
  0.0 84.4 jit_solution(16747108653619222627)
XLA Ops:
  0.0 0.0 copy-start.3
  0.0 1.0 %copy-done.3 = bf16[128,2048]{1,0:T(8,128)(2,1)S(1)} copy-done((bf16[128,2048]{1,0:T(8,128)(2,1)S(1)}, bf16[128,2048]{1,0:T(8,128)(2,1)}, u32[]{:S(2)}) %copy-start.3) | copy-done | bytes 524312
  1.0 0.0 copy-start.4
  1.0 0.7 copy-done.4
  1.7 0.0 copy-start.5
  1.7 0.7 copy-done.5
  2.4 0.0 copy-start.2
  2.4 0.6 dispatch.1
  3.0 0.0 copy-start
  3.0 0.0 copy-start.1
  3.0 42.1 %all_to_all.10.x_ref = bf16[128,4,2048]{2,1,0:T(4,128)(2,1)S(1)} all-to-all(bf16[128,4,2048]{2,1,0:T(4,128)(2,1)S(1)} %bitcast.7), channel_id=1, replica_groups=mesh['ep'=32,'tp'=4] {'ep','tp'}, dimensions={0} | all-to-all | bytes 4194304 | tf_op jit(solution)/shard_map/all_to_all | solution.py:84
  45.1 0.0 copy-done.2
  45.1 0.0 copy-done
  45.1 0.0 copy-done.1
  45.1 3.4 %expert.1 = bf16[128,4,2048]{2,1,0:T(4,128)(2,1)S(1)} custom-call(bf16[128,4,2048]{2,1,0:T(4,128)(2,1)S(1)} %all_to_all.10.x_ref, bf16[2048,512]{1,0:T(8,128)(2,1)S(1)} %bitcast.8, bf16[2048,512]{1,0:T(8,128)(2,1)S(1)} %bitcast.9, bf16[512,2048]{1,0:T(8,128)(2,1)S(1)} %bitcast.10), custom_call_target="tpu_custom_call" | custom-call | tf_op jit(solution)/shard_map/expert/pallas_call | solution.py:86
  48.6 0.0 copy-start.6
  48.6 0.0 copy-start.7
  48.6 34.2 %all_to_all.11.refs_0_ = bf16[128,4,2048]{2,1,0:T(4,128)(2,1)S(1)} all-to-all(bf16[128,4,2048]{2,1,0:T(4,128)(2,1)S(1)} %expert.1), channel_id=1, replica_groups=mesh['ep'=32,'tp'=4] {'ep','tp'}, dimensions={0} | all-to-all | bytes 4194304 | tf_op jit(solution)/shard_map/all_to_all | solution.py:94
  82.7 0.0 copy-done.6
  82.7 0.0 copy-done.7
  82.8 1.7 %combine.1 = bf16[128,2048]{1,0:T(8,128)(2,1)} custom-call(bf16[128,4,2048]{2,1,0:T(4,128)(2,1)S(1)} %all_to_all.11.refs_0_, s32[2,128]{1,0:T(2,128)S(1)} %bitcast.13, f32[2,128]{1,0:T(2,128)S(1)} %bitcast.14), custom_call_target="tpu_custom_call" | custom-call | tf_op jit(solution)/shard_map/combine/pallas_call | solution.py:95
Async XLA Ops:
  0.0 1.0 %copy-start.3 = (bf16[128,2048]{1,0:T(8,128)(2,1)S(1)}, bf16[128,2048]{1,0:T(8,128)(2,1)}, u32[]{:S(2)}) copy-start(bf16[128,2048]{1,0:T(8,128)(2,1)} %refs_0_.1) | copy-start | bytes 1572868
  1.0 0.7 copy-start.4
  1.7 0.7 copy-start.5
  2.4 42.7 %copy-start.2 = (bf16[1,512,2048]{2,1,0:T(8,128)(2,1)S(1)}, bf16[1,512,2048]{2,1,0:T(8,128)(2,1)}, u32[]{:S(2)}) copy-start(bf16[1,512,2048]{2,1,0:T(8,128)(2,1)} %param.11) | copy-start | bytes 6291460
  3.0 42.1 %copy-start = (bf16[1,2048,512]{2,1,0:T(8,128)(2,1)S(1)}, bf16[1,2048,512]{2,1,0:T(8,128)(2,1)}, u32[]{:S(2)}) copy-start(bf16[1,2048,512]{2,1,0:T(8,128)(2,1)} %param.9) | copy-start | bytes 6291460
  3.0 42.1 %copy-start.1 = (bf16[1,2048,512]{2,1,0:T(8,128)(2,1)S(1)}, bf16[1,2048,512]{2,1,0:T(8,128)(2,1)}, u32[]{:S(2)}) copy-start(bf16[1,2048,512]{2,1,0:T(8,128)(2,1)} %param.10) | copy-start | bytes 6291460
  48.6 34.2 %copy-start.6 = (s32[128,2]{0,1:T(2,128)S(1)}, s32[128,2]{0,1:T(2,128)}, u32[]{:S(2)}) copy-start(s32[128,2]{0,1:T(2,128)} %param.12) | copy-start | bytes 3076
  48.6 34.2 %copy-start.7 = (f32[128,2]{0,1:T(2,128)S(1)}, f32[128,2]{0,1:T(2,128)}, u32[]{:S(2)}) copy-start(f32[128,2]{0,1:T(2,128)} %param.13) | copy-start | bytes 3076

commit v3 on v2

v3 whole, which is shorter than its diff:
```python
import jax
import jax.numpy as jnp
from jax import lax
from jax.experimental import pallas as pl
from jax.experimental.pallas import tpu as pltpu
from jax.sharding import PartitionSpec as P

AXES = ("ep", "tp")
BF = jnp.bfloat16
F32 = jnp.float32


def rank_in_group(group, groups):
    n = group.shape[1]
    member = lax.broadcasted_iota(jnp.int32, (groups, n), 0) == group
    earlier = lax.broadcasted_iota(jnp.int32, (n, n), 0) < lax.broadcasted_iota(jnp.int32, (n, n), 1)
    counts = jnp.dot(member.astype(BF), earlier.astype(BF), preferred_element_type=F32)
    return jnp.sum(jnp.where(member, counts, 0.0), axis=0, keepdims=True).astype(jnp.int32)


def slots_kernel(groups, members, route_ref, pick_ref):
    rows = pick_ref.shape[0]
    group = route_ref[0:1, :] // members
    place = group * (rows // groups) + rank_in_group(group, groups)
    pick_ref[...] = (lax.broadcasted_iota(jnp.int32, (rows, rows), 0) == place).astype(BF)


def dispatch_kernel(groups, members, pick_ref, tok_ref, gain_ref, out_ref):
    rows, width = tok_ref.shape
    values = tok_ref[...].astype(F32)
    scale = lax.rsqrt(jnp.mean(values * values, axis=-1, keepdims=True) + 1e-06)
    normed = (values * scale * gain_ref[...]).astype(BF)
    ordered = jnp.dot(pick_ref[...], normed, preferred_element_type=F32).astype(BF)
    ordered = ordered.reshape(groups, rows // groups, width)
    for m in range(members):
        out_ref[:, m] = ordered


def selection(groups, members, slots, route_ref, gw_ref):
    rows = route_ref.shape[1]
    e0, e1 = route_ref[0:1, :], route_ref[1:2, :]
    rank = rank_in_group(e0 // members, groups)
    row = lax.broadcasted_iota(jnp.int32, (groups * members * slots, rows), 0)
    expert = row // slots
    weight = jnp.where(expert == e0, gw_ref[0:1, :], 0.0) + jnp.where(expert == e1, gw_ref[1:2, :], 0.0)
    weight = jnp.where(row % slots == rank, weight, 0.0).T
    high = weight.astype(BF)
    return jnp.concatenate([high, (weight - high.astype(F32)).astype(BF)], axis=0)


def expert_kernel(groups, members, x_ref, wg_ref, wu_ref, wd_ref, route_ref, gw_ref, out_ref, pick_ref):
    pick_ref[...] = selection(groups, members, x_ref.shape[1], route_ref, gw_ref)
    blocks, slots, width = x_ref.shape
    step = blocks // 2
    half = wg_ref.shape[1] // 2
    for c in range(2):
        x = x_ref[c * step:(c + 1) * step].reshape(step * slots, width)
        parts = []
        for n in range(2):
            gate = jnp.dot(x, wg_ref[:, n * half:(n + 1) * half], preferred_element_type=F32)
            up = jnp.dot(x, wu_ref[:, n * half:(n + 1) * half], preferred_element_type=F32)
            parts.append((gate / (1.0 + jnp.exp(-gate)) * up).astype(BF))
        hidden = jnp.concatenate(parts, axis=1)
        out = jnp.dot(hidden, wd_ref[...], preferred_element_type=F32).astype(BF)
        out_ref[c * step:(c + 1) * step] = out.reshape(step, slots, width)


def combine_kernel(r_ref, pick_ref, out_ref):
    blocks, slots, width = r_ref.shape
    rows = out_ref.shape[0]
    r = r_ref[...].reshape(blocks * slots, width)
    out = jnp.dot(pick_ref[...], r, preferred_element_type=F32)
    out_ref[...] = (out[:rows] + out[rows:]).astype(BF)


def local(tokens, norm_gain, w_gate, w_up, w_down, routing, gate_weight):
    rows, width = tokens.shape
    groups = lax.axis_size("ep")
    members = lax.axis_size("tp")
    experts = groups * members
    slots = rows // groups
    route = routing.T
    weights = gate_weight.T
    params = pltpu.CompilerParams(vmem_limit_bytes=20 * 1024 * 1024)
    pick = pl.pallas_call(
        lambda *refs: slots_kernel(groups, members, *refs),
        out_shape=jax.ShapeDtypeStruct((rows, rows), BF),
        compiler_params=params,
        cost_estimate=pl.CostEstimate(flops=2_000_000_000, bytes_accessed=0, transcendentals=0),
        name="slots",
    )(route)
    outgoing = pl.pallas_call(
        lambda *refs: dispatch_kernel(groups, members, *refs),
        out_shape=jax.ShapeDtypeStruct((groups, members, slots, width), BF),
        compiler_params=params,
        name="dispatch",
    )(pick, tokens, norm_gain.reshape(1, width))
    arrived = lax.all_to_all(outgoing.reshape(experts, slots, width), AXES, split_axis=0, concat_axis=0, tiled=True)
    in_vmem = pl.BlockSpec(memory_space=pltpu.VMEM)
    answered, weighted = pl.pallas_call(
        lambda *refs: expert_kernel(groups, members, *refs),
        in_specs=[in_vmem] * 6,
        out_specs=[in_vmem] * 2,
        out_shape=[
            jax.ShapeDtypeStruct((experts, slots, width), BF),
            jax.ShapeDtypeStruct((2 * rows, experts * slots), BF),
        ],
        compiler_params=params,
        name="expert",
    )(arrived, w_gate[0], w_up[0], w_down[0], route, weights)
    returned = lax.all_to_all(answered, AXES, split_axis=0, concat_axis=0, tiled=True)
    return pl.pallas_call(
        combine_kernel,
        out_shape=jax.ShapeDtypeStruct((rows, width), BF),
        compiler_params=params,
        name="combine",
    )(returned, weighted)


def solution(mesh):
    placed = (
        P(AXES, None),
        P(),
        P(AXES, None, None),
        P(AXES, None, None),
        P(AXES, None, None),
        P(AXES, None),
        P(AXES, None),
    )
    return jax.shard_map(local, mesh=mesh, in_specs=placed, out_specs=P(AXES, None), check_vma=False)
```

time: 84.7 us -> 83.8 us (0.989)
  local copies, waits for them, and re-layouts: 2.44 us -> 1.59 us
    unnamed x16 -> x14, local copies, waits for them, and re-layouts: 2.44 us -> 1.59 us
    pallas_call x2 -> x3, Pallas kernels: 5.13 us -> 5.16 us  [the longest x1 3.49 us: local(): pl.pallas_call(lambda *refs: expert_kernel(groups, members, *refs), in_sp...]
where the time goes in v3:
time: 83.8 us; the launch traced here: 83.6 us
  blocking collectives  76.2 us (91%)
  Pallas kernels  5.75 us (7%)
  local copies, waits for them, and re-layouts  1.59 us (2%)
    all_to_all x1, blocking collectives, local(): lax.all_to_all(outgoing.reshape(experts, slots, width), AXES, split_axis=...  42.1 us
    all_to_all x1, blocking collectives, local(): lax.all_to_all(answered, AXES, split_axis=0, concat_axis=0, tiled=True)  34.2 us
    pallas_call x1, Pallas kernels, local(): pl.pallas_call(lambda *refs: expert_kernel(groups, members, *refs), in_sp...  3.49 us

profile of v3, /device:TPU:1, one launch (start us, length us, event | category | flops | bytes accessed | tf_op | source)
XLA Modules:
  0.0 83.6 jit_solution(9061865274642699769)
XLA Ops:
  0.0 0.0 copy-start.5
  0.0 0.7 copy-done.5
  0.7 0.0 copy-start.3
  0.7 0.0 copy-start.4
  0.7 0.2 slots.1.refs_0_
  0.8 0.9 %copy-done.3 = bf16[128,2048]{1,0:T(8,128)(2,1)S(1)} copy-done((bf16[128,2048]{1,0:T(8,128)(2,1)S(1)}, bf16[128,2048]{1,0:T(8,128)(2,1)}, u32[]{:S(2)}) %copy-start.3) | copy-done | bytes 524312
  1.7 0.0 copy-done.4
  1.7 0.0 copy-start.2
  1.7 0.6 dispatch.1
  2.3 0.0 copy-start
  2.3 0.0 copy-start.1
  2.3 0.0 copy-start.6
  2.4 42.1 %all_to_all.10.refs_0_ = bf16[128,4,2048]{2,1,0:T(4,128)(2,1)S(1)} all-to-all(bf16[128,4,2048]{2,1,0:T(4,128)(2,1)S(1)} %bitcast.7), channel_id=1, replica_groups=mesh['ep'=32,'tp'=4] {'ep','tp'}, dimensions={0} | all-to-all | bytes 4194304 | tf_op jit(solution)/shard_map/all_to_all | solution.py:98
  44.4 0.0 copy-done.2
  44.4 0.0 copy-done
  44.4 0.0 copy-done.1
  44.4 0.0 copy-done.6
  44.4 3.5 %expert.1 = (bf16[128,4,2048]{2,1,0:T(4,128)(2,1)S(1)}, bf16[256,512]{1,0:T(8,128)(2,1)S(1)}) custom-call(bf16[128,4,2048]{2,1,0:T(4,128)(2,1)S(1)} %all_to_all.10.refs_0_, bf16[2048,512]{1,0:T(8,128)(2,1)S(1)} %bitcast.8, bf16[2048,512]{1,0:T(8,128)(2,1)S(1)} %bitcast.9, bf16[512,2048]{1,0:T(8,128)(2,1)S(1)} %bitcast.10, s32[2,128]{1,0:T(2,128)S(1)} %bitcast.13, ...), custom_call_target="tpu_custom_call" | custom-call | tf_op jit(solution)/shard_map/expert/pallas_call | solution.py:100
  47.9 34.2 %all_to_all.11.r_ref = bf16[128,4,2048]{2,1,0:T(4,128)(2,1)S(1)} all-to-all(bf16[128,4,2048]{2,1,0:T(4,128)(2,1)S(1)} %get-tuple-element.7), channel_id=1, replica_groups=mesh['ep'=32,'tp'=4] {'ep','tp'}, dimensions={0} | all-to-all | bytes 4194304 | tf_op jit(solution)/shard_map/all_to_all | solution.py:111
  82.1 1.5 %combine.1 = bf16[128,2048]{1,0:T(8,128)(2,1)} custom-call(bf16[128,4,2048]{2,1,0:T(4,128)(2,1)S(1)} %all_to_all.11.r_ref, bf16[256,512]{1,0:T(8,128)(2,1)S(1)} %get-tuple-element.8.pick_ref), custom_call_target="tpu_custom_call" | custom-call | tf_op jit(solution)/shard_map/combine/pallas_call | solution.py:112
Async XLA Ops:
  0.0 0.7 copy-start.5
  0.7 1.0 %copy-start.3 = (bf16[128,2048]{1,0:T(8,128)(2,1)S(1)}, bf16[128,2048]{1,0:T(8,128)(2,1)}, u32[]{:S(2)}) copy-start(bf16[128,2048]{1,0:T(8,128)(2,1)} %refs_1_.1) | copy-start | bytes 1572868
  0.7 1.0 %copy-start.4 = (f32[2048]{0:T(1024)S(1)}, f32[2048]{0:T(1024)}, u32[]{:S(2)}) copy-start(f32[2048]{0:T(1024)} %param.8) | copy-start | bytes 24580
  1.7 42.7 %copy-start.2 = (bf16[1,512,2048]{2,1,0:T(8,128)(2,1)S(1)}, bf16[1,512,2048]{2,1,0:T(8,128)(2,1)}, u32[]{:S(2)}) copy-start(bf16[1,512,2048]{2,1,0:T(8,128)(2,1)} %param.11) | copy-start | bytes 6291460
  2.3 42.1 %copy-start = (bf16[1,2048,512]{2,1,0:T(8,128)(2,1)S(1)}, bf16[1,2048,512]{2,1,0:T(8,128)(2,1)}, u32[]{:S(2)}) copy-start(bf16[1,2048,512]{2,1,0:T(8,128)(2,1)} %param.9) | copy-start | bytes 6291460
  2.3 42.1 %copy-start.1 = (bf16[1,2048,512]{2,1,0:T(8,128)(2,1)S(1)}, bf16[1,2048,512]{2,1,0:T(8,128)(2,1)}, u32[]{:S(2)}) copy-start(bf16[1,2048,512]{2,1,0:T(8,128)(2,1)} %param.10) | copy-start | bytes 6291460
  2.3 42.1 %copy-start.6 = (f32[128,2]{0,1:T(2,128)S(1)}, f32[128,2]{0,1:T(2,128)}, u32[]{:S(2)}) copy-start(f32[128,2]{0,1:T(2,128)} %param.13) | copy-start | bytes 3076

commit v4 on v3

--- a/solution.py
+++ b/solution.py
@@ -18,9 +18,13 @@
     return jnp.sum(jnp.where(member, counts, 0.0), axis=0, keepdims=True).astype(jnp.int32)
 
 
-def slots_kernel(groups, members, route_ref, pick_ref):
+def lead_kernel(out_ref):
+    out_ref[...] = jnp.zeros(out_ref.shape, jnp.int32)
+
+
+def slots_kernel(groups, members, zero_ref, route_ref, pick_ref):
     rows = pick_ref.shape[0]
-    group = route_ref[0:1, :] // members
+    group = (route_ref[0:1, :] + zero_ref[0:1, :]) // members
     place = group * (rows // groups) + rank_in_group(group, groups)
     pick_ref[...] = (lax.broadcasted_iota(jnp.int32, (rows, rows), 0) == place).astype(BF)
 
@@ -65,12 +69,22 @@
         out_ref[c * step:(c + 1) * step] = out.reshape(step, slots, width)
 
 
-def combine_kernel(r_ref, pick_ref, out_ref):
+def combine_kernel(r_ref, pick_ref, out_hbm, out_ref, sems):
     blocks, slots, width = r_ref.shape
     rows = out_ref.shape[0]
-    r = r_ref[...].reshape(blocks * slots, width)
-    out = jnp.dot(pick_ref[...], r, preferred_element_type=F32)
-    out_ref[...] = (out[:rows] + out[rows:]).astype(BF)
+    parts = sems.shape[0]
+    step = width // parts
+    pick = pick_ref[...]
+    copies = []
+    for p in range(parts):
+        span = pl.ds(p * step, step)
+        r = r_ref[:, :, p * step:(p + 1) * step].reshape(blocks * slots, step)
+        out = jnp.dot(pick, r, preferred_element_type=F32)
+        out_ref[:, p * step:(p + 1) * step] = (out[:rows] + out[rows:]).astype(BF)
+        copies.append(pltpu.make_async_copy(out_ref.at[:, span], out_hbm.at[:, span], sems.at[p]))
+        copies[-1].start()
+    for copy in copies:
+        copy.wait()
 
 
 def local(tokens, norm_gain, w_gate, w_up, w_down, routing, gate_weight):
@@ -82,13 +96,20 @@
     route = routing.T
     weights = gate_weight.T
     params = pltpu.CompilerParams(vmem_limit_bytes=20 * 1024 * 1024)
+    busy = pl.CostEstimate(flops=2_000_000_000, bytes_accessed=0, transcendentals=0)
+    zero = pl.pallas_call(
+        lead_kernel,
+        out_shape=jax.ShapeDtypeStruct((8, rows), jnp.int32),
+        compiler_params=params,
+        cost_estimate=busy,
+        name="lead",
+    )()
     pick = pl.pallas_call(
         lambda *refs: slots_kernel(groups, members, *refs),
         out_shape=jax.ShapeDtypeStruct((rows, rows), BF),
         compiler_params=params,
-        cost_estimate=pl.CostEstimate(flops=2_000_000_000, bytes_accessed=0, transcendentals=0),
         name="slots",
-    )(route)
+    )(zero, route)
     outgoing = pl.pallas_call(
         lambda *refs: dispatch_kernel(groups, members, *refs),
         out_shape=jax.ShapeDtypeStruct((groups, members, slots, width), BF),
@@ -111,7 +132,10 @@
     returned = lax.all_to_all(answered, AXES, split_axis=0, concat_axis=0, tiled=True)
     return pl.pallas_call(
         combine_kernel,
+        in_specs=[in_vmem] * 2,
+        out_specs=pl.BlockSpec(memory_space=pltpu.HBM),
         out_shape=jax.ShapeDtypeStruct((rows, width), BF),
+        scratch_shapes=[pltpu.VMEM((rows, width), BF), pltpu.SemaphoreType.DMA((4,))],
         compiler_params=params,
         name="combine",
     )(returned, weighted)

time: 83.8 us -> 83 us (level)
  no operation moved by 1% of the time
where the time goes in v4:
time: 83 us; the launch traced here: 82.9 us
  blocking collectives  76.2 us (92%)
  Pallas kernels  5.66 us (7%)
  local copies, waits for them, and re-layouts  0.92 us (1%)
    all_to_all x1, blocking collectives, local(): lax.all_to_all(outgoing.reshape(experts, slots, width), AXES, split_axis=...  42.1 us
    all_to_all x1, blocking collectives, local(): lax.all_to_all(answered, AXES, split_axis=0, concat_axis=0, tiled=True)  34.2 us
    pallas_call x1, Pallas kernels, local(): pl.pallas_call(lambda *refs: expert_kernel(groups, members, *refs), in_sp...  3.49 us

profile of v4, /device:TPU:1, one launch (start us, length us, event | category | flops | bytes accessed | tf_op | source)
XLA Modules:
  0.0 82.9 jit_solution(8905923168520402416)
XLA Ops:
  0.0 0.0 copy-start.5
  0.0 0.0 copy-start.4
  0.0 0.0 copy-start.3
  0.0 0.7 copy-done.5
  0.7 0.2 slots.1.refs_0_
  0.8 0.0 copy-done.4
  0.8 0.2 copy-done.3
  1.1 0.0 copy-start.2
  1.1 0.6 dispatch.1
  1.7 0.0 copy-start
  1.7 0.0 copy-start.1
  1.7 0.0 copy-start.6
  1.7 42.1 %all_to_all.10.refs_0_ = bf16[128,4,2048]{2,1,0:T(4,128)(2,1)S(1)} all-to-all(bf16[128,4,2048]{2,1,0:T(4,128)(2,1)S(1)} %bitcast.7), channel_id=1, replica_groups=mesh['ep'=32,'tp'=4] {'ep','tp'}, dimensions={0} | all-to-all | bytes 4194304 | tf_op jit(solution)/shard_map/all_to_all | solution.py:119
  43.8 0.0 copy-done.2
  43.8 0.0 copy-done
  43.8 0.0 copy-done.1
  43.8 0.0 copy-done.6
  43.8 3.5 %expert.1 = (bf16[128,4,2048]{2,1,0:T(4,128)(2,1)S(1)}, bf16[256,512]{1,0:T(8,128)(2,1)S(1)}) custom-call(bf16[128,4,2048]{2,1,0:T(4,128)(2,1)S(1)} %all_to_all.10.refs_0_, bf16[2048,512]{1,0:T(8,128)(2,1)S(1)} %bitcast.8, bf16[2048,512]{1,0:T(8,128)(2,1)S(1)} %bitcast.9, bf16[512,2048]{1,0:T(8,128)(2,1)S(1)} %bitcast.10, s32[2,128]{1,0:T(2,128)S(1)} %bitcast.13, ...), custom_call_target="tpu_custom_call" | custom-call | tf_op jit(solution)/shard_map/expert/pallas_call | solution.py:121
  47.3 34.2 %all_to_all.11.r_ref = bf16[128,4,2048]{2,1,0:T(4,128)(2,1)S(1)} all-to-all(bf16[128,4,2048]{2,1,0:T(4,128)(2,1)S(1)} %get-tuple-element.7), channel_id=1, replica_groups=mesh['ep'=32,'tp'=4] {'ep','tp'}, dimensions={0} | all-to-all | bytes 4194304 | tf_op jit(solution)/shard_map/all_to_all | solution.py:132
  81.4 1.4 %combine.1 = bf16[128,2048]{1,0:T(8,128)(2,1)} custom-call(bf16[128,4,2048]{2,1,0:T(4,128)(2,1)S(1)} %all_to_all.11.r_ref, bf16[256,512]{1,0:T(8,128)(2,1)S(1)} %get-tuple-element.8.pick_ref), custom_call_target="tpu_custom_call" | custom-call | tf_op jit(solution)/shard_map/combine/pallas_call | solution.py:133
  (1 shorter events, 0.0 us)
Async XLA Ops:
  0.0 0.7 copy-start.5
  0.0 0.8 %copy-start.4 = (f32[2048]{0:T(1024)S(1)}, f32[2048]{0:T(1024)}, u32[]{:S(2)}) copy-start(f32[2048]{0:T(1024)} %param.8) | copy-start | bytes 24580
  0.0 1.1 %copy-start.3 = (bf16[128,2048]{1,0:T(8,128)(2,1)S(1)}, bf16[128,2048]{1,0:T(8,128)(2,1)}, u32[]{:S(2)}) copy-start(bf16[128,2048]{1,0:T(8,128)(2,1)} %refs_1_.1) | copy-start | bytes 1572868
  1.1 42.7 %copy-start.2 = (bf16[1,512,2048]{2,1,0:T(8,128)(2,1)S(1)}, bf16[1,512,2048]{2,1,0:T(8,128)(2,1)}, u32[]{:S(2)}) copy-start(bf16[1,512,2048]{2,1,0:T(8,128)(2,1)} %param.11) | copy-start | bytes 6291460
  1.7 42.1 %copy-start = (bf16[1,2048,512]{2,1,0:T(8,128)(2,1)S(1)}, bf16[1,2048,512]{2,1,0:T(8,128)(2,1)}, u32[]{:S(2)}) copy-start(bf16[1,2048,512]{2,1,0:T(8,128)(2,1)} %param.9) | copy-start | bytes 6291460
  1.7 42.1 %copy-start.1 = (bf16[1,2048,512]{2,1,0:T(8,128)(2,1)S(1)}, bf16[1,2048,512]{2,1,0:T(8,128)(2,1)}, u32[]{:S(2)}) copy-start(bf16[1,2048,512]{2,1,0:T(8,128)(2,1)} %param.10) | copy-start | bytes 6291460
  1.7 42.1 %copy-start.6 = (f32[128,2]{0,1:T(2,128)S(1)}, f32[128,2]{0,1:T(2,128)}, u32[]{:S(2)}) copy-start(f32[128,2]{0,1:T(2,128)} %param.13) | copy-start | bytes 3076

commit v5 on v4

--- a/solution.py
+++ b/solution.py
@@ -18,26 +18,29 @@
     return jnp.sum(jnp.where(member, counts, 0.0), axis=0, keepdims=True).astype(jnp.int32)
 
 
-def lead_kernel(out_ref):
-    out_ref[...] = jnp.zeros(out_ref.shape, jnp.int32)
-
-
-def slots_kernel(groups, members, zero_ref, route_ref, pick_ref):
-    rows = pick_ref.shape[0]
-    group = (route_ref[0:1, :] + zero_ref[0:1, :]) // members
-    place = group * (rows // groups) + rank_in_group(group, groups)
-    pick_ref[...] = (lax.broadcasted_iota(jnp.int32, (rows, rows), 0) == place).astype(BF)
-
-
-def dispatch_kernel(groups, members, pick_ref, tok_ref, gain_ref, out_ref):
+def dispatch_kernel(groups, members, tok_hbm, gain_hbm, route_hbm, out_ref, tok_ref, gain_ref, route_ref, sems):
     rows, width = tok_ref.shape
-    values = tok_ref[...].astype(F32)
-    scale = lax.rsqrt(jnp.mean(values * values, axis=-1, keepdims=True) + 1e-06)
-    normed = (values * scale * gain_ref[...]).astype(BF)
-    ordered = jnp.dot(pick_ref[...], normed, preferred_element_type=F32).astype(BF)
-    ordered = ordered.reshape(groups, rows // groups, width)
-    for m in range(members):
-        out_ref[:, m] = ordered
+    slots = rows // groups
+    copies = [
+        pltpu.make_async_copy(route_hbm, route_ref, sems.at[0]),
+        pltpu.make_async_copy(tok_hbm, tok_ref, sems.at[1]),
+        pltpu.make_async_copy(gain_hbm, gain_ref, sems.at[2]),
+    ]
+    for copy in copies:
+        copy.start()
+    copies[0].wait()
+    group = route_ref[0:1, :] // members
+    place = group * slots + rank_in_group(group, groups)
+    pick = (lax.broadcasted_iota(jnp.int32, (rows, rows), 0) == place).astype(BF)
+    copies[1].wait()
+    copies[2].wait()
+    half = rows // 2
+    for c in range(2):
+        values = jnp.dot(pick[c * half:(c + 1) * half], tok_ref[...], preferred_element_type=F32)
+        scale = lax.rsqrt(jnp.mean(values * values, axis=-1, keepdims=True) + 1e-06)
+        normed = (values * scale * gain_ref[...]).astype(BF).reshape(groups // 2, slots, width)
+        for m in range(members):
+            out_ref[c * groups // 2:(c + 1) * groups // 2, m] = normed
 
 
 def selection(groups, members, slots, route_ref, gw_ref):
@@ -96,28 +99,24 @@
     route = routing.T
     weights = gate_weight.T
     params = pltpu.CompilerParams(vmem_limit_bytes=20 * 1024 * 1024)
-    busy = pl.CostEstimate(flops=2_000_000_000, bytes_accessed=0, transcendentals=0)
-    zero = pl.pallas_call(
-        lead_kernel,
-        out_shape=jax.ShapeDtypeStruct((8, rows), jnp.int32),
-        compiler_params=params,
-        cost_estimate=busy,
-        name="lead",
-    )()
-    pick = pl.pallas_call(
-        lambda *refs: slots_kernel(groups, members, *refs),
-        out_shape=jax.ShapeDtypeStruct((rows, rows), BF),
-        compiler_params=params,
-        name="slots",
-    )(zero, route)
+    in_vmem = pl.BlockSpec(memory_space=pltpu.VMEM)
+    in_hbm = pl.BlockSpec(memory_space=pltpu.HBM)
+    sources = [pltpu.with_memory_space_constraint(v, pltpu.HBM) for v in (tokens, norm_gain.reshape(1, width), route)]
     outgoing = pl.pallas_call(
         lambda *refs: dispatch_kernel(groups, members, *refs),
+        in_specs=[in_hbm] * 3,
+        out_specs=in_vmem,
         out_shape=jax.ShapeDtypeStruct((groups, members, slots, width), BF),
+        scratch_shapes=[
+            pltpu.VMEM((rows, width), BF),
+            pltpu.VMEM((1, width), F32),
+            pltpu.VMEM(route.shape, jnp.int32),
+            pltpu.SemaphoreType.DMA((3,)),
+        ],
         compiler_params=params,
         name="dispatch",
-    )(pick, tokens, norm_gain.reshape(1, width))
+    )(*sources)
     arrived = lax.all_to_all(outgoing.reshape(experts, slots, width), AXES, split_axis=0, concat_axis=0, tiled=True)
-    in_vmem = pl.BlockSpec(memory_space=pltpu.VMEM)
     answered, weighted = pl.pallas_call(
         lambda *refs: expert_kernel(groups, members, *refs),
         in_specs=[in_vmem] * 6,

time: 83 us -> 83.1 us (level)
  Pallas kernels: 5.66 us -> 6.63 us
  local copies, waits for them, and re-layouts: 0.92 us -> 0.03 us
    pallas_call x3 -> x1, Pallas kernels: 0.74 us -> 1.71 us  [local(): pl.pallas_call(lambda *refs: dispatch_kernel(groups, members, *refs), in_...]
    unnamed x14 -> x10, local copies, waits for them, and re-layouts: 0.92 us -> 0.03 us
where the time goes in v5:
time: 83.1 us; the launch traced here: 82.9 us
  blocking collectives  76.2 us (92%)
  Pallas kernels  6.63 us (8%)
    all_to_all x1, blocking collectives, local(): lax.all_to_all(outgoing.reshape(experts, slots, width), AXES, split_axis=...  42 us
    all_to_all x1, blocking collectives, local(): lax.all_to_all(answered, AXES, split_axis=0, concat_axis=0, tiled=True)  34.2 us
    pallas_call x1, Pallas kernels, local(): pl.pallas_call(lambda *refs: expert_kernel(groups, members, *refs), in_sp...  3.49 us
    pallas_call x1, Pallas kernels, local(): pl.pallas_call(lambda *refs: dispatch_kernel(groups, members, *refs), in_...  1.71 us

profile of v5, /device:TPU:1, one launch (start us, length us, event | category | flops | bytes accessed | tf_op | source)
XLA Modules:
  0.0 82.9 jit_solution(3332030986235529863)
XLA Ops:
  0.0 0.0 copy-start.2
  0.0 1.7 %dispatch.1 = bf16[32,4,4,2048]{3,2,1,0:T(4,128)(2,1)S(1)} custom-call(bf16[128,2048]{1,0:T(8,128)(2,1)} %refs_0_.1, f32[1,2048]{1,0:T(1,128)} %bitcast.14, s32[2,128]{1,0:T(2,128)} %bitcast.11), custom_call_target="tpu_custom_call" | custom-call | tf_op jit(solution)/shard_map/dispatch/pallas_call | solution.py:105
  1.7 0.0 copy-start
  1.7 0.0 copy-start.1
  1.7 0.0 copy-start.3
  1.8 0.0 copy-start.4
  1.8 42.0 %all_to_all.10.refs_0_ = bf16[128,4,2048]{2,1,0:T(4,128)(2,1)S(1)} all-to-all(bf16[128,4,2048]{2,1,0:T(4,128)(2,1)S(1)} %bitcast.7), channel_id=1, replica_groups=mesh['ep'=32,'tp'=4] {'ep','tp'}, dimensions={0} | all-to-all | bytes 4194304 | tf_op jit(solution)/shard_map/all_to_all | solution.py:119
  43.8 0.0 copy-done.2
  43.8 0.0 copy-done
  43.8 0.0 copy-done.1
  43.8 0.0 copy-done.3
  43.8 0.0 copy-done.4
  43.8 3.5 %expert.1 = (bf16[128,4,2048]{2,1,0:T(4,128)(2,1)S(1)}, bf16[256,512]{1,0:T(8,128)(2,1)S(1)}) custom-call(bf16[128,4,2048]{2,1,0:T(4,128)(2,1)S(1)} %all_to_all.10.refs_0_, bf16[2048,512]{1,0:T(8,128)(2,1)S(1)} %bitcast.8, bf16[2048,512]{1,0:T(8,128)(2,1)S(1)} %bitcast.9, bf16[512,2048]{1,0:T(8,128)(2,1)S(1)} %bitcast.10, s32[2,128]{1,0:T(2,128)S(1)} %bitcast.12, ...), custom_call_target="tpu_custom_call" | custom-call | tf_op jit(solution)/shard_map/expert/pallas_call | solution.py:120
  47.3 34.2 %all_to_all.11.r_ref = bf16[128,4,2048]{2,1,0:T(4,128)(2,1)S(1)} all-to-all(bf16[128,4,2048]{2,1,0:T(4,128)(2,1)S(1)} %get-tuple-element.7), channel_id=1, replica_groups=mesh['ep'=32,'tp'=4] {'ep','tp'}, dimensions={0} | all-to-all | bytes 4194304 | tf_op jit(solution)/shard_map/all_to_all | solution.py:131
  81.5 1.4 %combine.1 = bf16[128,2048]{1,0:T(8,128)(2,1)} custom-call(bf16[128,4,2048]{2,1,0:T(4,128)(2,1)S(1)} %all_to_all.11.r_ref, bf16[256,512]{1,0:T(8,128)(2,1)S(1)} %get-tuple-element.8.pick_ref), custom_call_target="tpu_custom_call" | custom-call | tf_op jit(solution)/shard_map/combine/pallas_call | solution.py:132
Async XLA Ops:
  0.0 43.8 %copy-start.2 = (bf16[1,512,2048]{2,1,0:T(8,128)(2,1)S(1)}, bf16[1,512,2048]{2,1,0:T(8,128)(2,1)}, u32[]{:S(2)}) copy-start(bf16[1,512,2048]{2,1,0:T(8,128)(2,1)} %param.11) | copy-start | bytes 6291460
  1.7 42.1 %copy-start = (bf16[1,2048,512]{2,1,0:T(8,128)(2,1)S(1)}, bf16[1,2048,512]{2,1,0:T(8,128)(2,1)}, u32[]{:S(2)}) copy-start(bf16[1,2048,512]{2,1,0:T(8,128)(2,1)} %param.9) | copy-start | bytes 6291460
  1.7 42.1 %copy-start.1 = (bf16[1,2048,512]{2,1,0:T(8,128)(2,1)S(1)}, bf16[1,2048,512]{2,1,0:T(8,128)(2,1)}, u32[]{:S(2)}) copy-start(bf16[1,2048,512]{2,1,0:T(8,128)(2,1)} %param.10) | copy-start | bytes 6291460
  1.7 42.1 %copy-start.3 = (s32[128,2]{0,1:T(2,128)S(1)}, s32[128,2]{0,1:T(2,128)}, u32[]{:S(2)}) copy-start(s32[128,2]{0,1:T(2,128)} %param.12) | copy-start | bytes 3076
  1.8 42.1 %copy-start.4 = (f32[128,2]{0,1:T(2,128)S(1)}, f32[128,2]{0,1:T(2,128)}, u32[]{:S(2)}) copy-start(f32[128,2]{0,1:T(2,128)} %param.13) | copy-start | bytes 3076

commit v6 on v4

--- a/solution.py
+++ b/solution.py
@@ -31,13 +31,13 @@
 
 def dispatch_kernel(groups, members, pick_ref, tok_ref, gain_ref, out_ref):
     rows, width = tok_ref.shape
-    values = tok_ref[...].astype(F32)
-    scale = lax.rsqrt(jnp.mean(values * values, axis=-1, keepdims=True) + 1e-06)
-    normed = (values * scale * gain_ref[...]).astype(BF)
-    ordered = jnp.dot(pick_ref[...], normed, preferred_element_type=F32).astype(BF)
-    ordered = ordered.reshape(groups, rows // groups, width)
-    for m in range(members):
-        out_ref[:, m] = ordered
+    half = rows // 2
+    for c in range(2):
+        values = jnp.dot(pick_ref[c * half:(c + 1) * half], tok_ref[...], preferred_element_type=F32)
+        scale = lax.rsqrt(jnp.mean(values * values, axis=-1, keepdims=True) + 1e-06)
+        normed = (values * scale * gain_ref[...]).astype(BF).reshape(groups // 2, rows // groups, width)
+        for m in range(members):
+            out_ref[c * groups // 2:(c + 1) * groups // 2, m] = normed
 
 
 def selection(groups, members, slots, route_ref, gw_ref):

time: 83 us -> 82.9 us (level)
  no operation moved by 1% of the time
where the time goes in v6:
time: 82.9 us; the launch traced here: 82.8 us
  blocking collectives  76.2 us (92%)
  Pallas kernels  5.55 us (7%)
  local copies, waits for them, and re-layouts  0.92 us (1%)
    all_to_all x1, blocking collectives, local(): lax.all_to_all(outgoing.reshape(experts, slots, width), AXES, split_axis=...  42.1 us
    all_to_all x1, blocking collectives, local(): lax.all_to_all(answered, AXES, split_axis=0, concat_axis=0, tiled=True)  34.2 us
    pallas_call x1, Pallas kernels, local(): pl.pallas_call(lambda *refs: expert_kernel(groups, members, *refs), in_sp...  3.49 us

profile of v6, /device:TPU:1, one launch (start us, length us, event | category | flops | bytes accessed | tf_op | source)
XLA Modules:
  0.0 82.8 jit_solution(5412381505544683164)
XLA Ops:
  0.0 0.0 copy-start.5
  0.0 0.0 copy-start.4
  0.0 0.0 copy-start.3
  0.0 0.7 copy-done.5
  0.7 0.2 slots.1.refs_0_
  0.8 0.0 copy-done.4
  0.8 0.2 copy-done.3
  1.1 0.0 copy-start.2
  1.1 0.5 dispatch.1
  1.6 0.0 copy-start
  1.6 0.0 copy-start.1
  1.6 0.0 copy-start.6
  1.6 42.1 %all_to_all.10.refs_0_ = bf16[128,4,2048]{2,1,0:T(4,128)(2,1)S(1)} all-to-all(bf16[128,4,2048]{2,1,0:T(4,128)(2,1)S(1)} %bitcast.7), channel_id=1, replica_groups=mesh['ep'=32,'tp'=4] {'ep','tp'}, dimensions={0} | all-to-all | bytes 4194304 | tf_op jit(solution)/shard_map/all_to_all | solution.py:119
  43.6 0.0 copy-done.2
  43.7 0.0 copy-done
  43.7 0.0 copy-done.1
  43.7 0.0 copy-done.6
  43.7 3.5 %expert.1 = (bf16[128,4,2048]{2,1,0:T(4,128)(2,1)S(1)}, bf16[256,512]{1,0:T(8,128)(2,1)S(1)}) custom-call(bf16[128,4,2048]{2,1,0:T(4,128)(2,1)S(1)} %all_to_all.10.refs_0_, bf16[2048,512]{1,0:T(8,128)(2,1)S(1)} %bitcast.8, bf16[2048,512]{1,0:T(8,128)(2,1)S(1)} %bitcast.9, bf16[512,2048]{1,0:T(8,128)(2,1)S(1)} %bitcast.10, s32[2,128]{1,0:T(2,128)S(1)} %bitcast.13, ...), custom_call_target="tpu_custom_call" | custom-call | tf_op jit(solution)/shard_map/expert/pallas_call | solution.py:121
  47.2 34.2 %all_to_all.11.r_ref = bf16[128,4,2048]{2,1,0:T(4,128)(2,1)S(1)} all-to-all(bf16[128,4,2048]{2,1,0:T(4,128)(2,1)S(1)} %get-tuple-element.7), channel_id=1, replica_groups=mesh['ep'=32,'tp'=4] {'ep','tp'}, dimensions={0} | all-to-all | bytes 4194304 | tf_op jit(solution)/shard_map/all_to_all | solution.py:132
  81.3 1.4 %combine.1 = bf16[128,2048]{1,0:T(8,128)(2,1)} custom-call(bf16[128,4,2048]{2,1,0:T(4,128)(2,1)S(1)} %all_to_all.11.r_ref, bf16[256,512]{1,0:T(8,128)(2,1)S(1)} %get-tuple-element.8.pick_ref), custom_call_target="tpu_custom_call" | custom-call | tf_op jit(solution)/shard_map/combine/pallas_call | solution.py:133
  (1 shorter events, 0.0 us)
Async XLA Ops:
  0.0 0.7 copy-start.5
  0.0 0.8 %copy-start.4 = (f32[2048]{0:T(1024)S(1)}, f32[2048]{0:T(1024)}, u32[]{:S(2)}) copy-start(f32[2048]{0:T(1024)} %param.8) | copy-start | bytes 24580
  0.0 1.1 %copy-start.3 = (bf16[128,2048]{1,0:T(8,128)(2,1)S(1)}, bf16[128,2048]{1,0:T(8,128)(2,1)}, u32[]{:S(2)}) copy-start(bf16[128,2048]{1,0:T(8,128)(2,1)} %refs_1_.1) | copy-start | bytes 1572868
  1.1 42.6 %copy-start.2 = (bf16[1,512,2048]{2,1,0:T(8,128)(2,1)S(1)}, bf16[1,512,2048]{2,1,0:T(8,128)(2,1)}, u32[]{:S(2)}) copy-start(bf16[1,512,2048]{2,1,0:T(8,128)(2,1)} %param.11) | copy-start | bytes 6291460
  1.6 42.1 %copy-start = (bf16[1,2048,512]{2,1,0:T(8,128)(2,1)S(1)}, bf16[1,2048,512]{2,1,0:T(8,128)(2,1)}, u32[]{:S(2)}) copy-start(bf16[1,2048,512]{2,1,0:T(8,128)(2,1)} %param.9) | copy-start | bytes 6291460
  1.6 42.1 %copy-start.1 = (bf16[1,2048,512]{2,1,0:T(8,128)(2,1)S(1)}, bf16[1,2048,512]{2,1,0:T(8,128)(2,1)}, u32[]{:S(2)}) copy-start(bf16[1,2048,512]{2,1,0:T(8,128)(2,1)} %param.10) | copy-start | bytes 6291460
  1.6 42.1 %copy-start.6 = (f32[128,2]{0,1:T(2,128)S(1)}, f32[128,2]{0,1:T(2,128)}, u32[]{:S(2)}) copy-start(f32[128,2]{0,1:T(2,128)} %param.13) | copy-start | bytes 3076

commit v7 on v6

--- a/solution.py
+++ b/solution.py
@@ -3,9 +3,11 @@
 from jax import lax
 from jax.experimental import pallas as pl
 from jax.experimental.pallas import tpu as pltpu
-from jax.sharding import PartitionSpec as P
+from jax.sharding import Mesh, PartitionSpec as P
 
-AXES = ("ep", "tp")
+AXES = ("chip", "core", "tp")
+ORDER = ("core", "chip", "tp")
+CORES = 2
 BF = jnp.bfloat16
 F32 = jnp.float32
 
@@ -22,10 +24,11 @@
     out_ref[...] = jnp.zeros(out_ref.shape, jnp.int32)
 
 
-def slots_kernel(groups, members, zero_ref, route_ref, pick_ref):
+def slots_kernel(groups, members, cores, zero_ref, route_ref, pick_ref):
     rows = pick_ref.shape[0]
     group = (route_ref[0:1, :] + zero_ref[0:1, :]) // members
-    place = group * (rows // groups) + rank_in_group(group, groups)
+    block = group % cores * (groups // cores) + group // cores
+    place = block * (rows // groups) + rank_in_group(group, groups)
     pick_ref[...] = (lax.broadcasted_iota(jnp.int32, (rows, rows), 0) == place).astype(BF)
 
 
@@ -40,20 +43,22 @@
             out_ref[c * groups // 2:(c + 1) * groups // 2, m] = normed
 
 
-def selection(groups, members, slots, route_ref, gw_ref):
+def selection(groups, members, cores, slots, route_ref, gw_ref):
     rows = route_ref.shape[1]
     e0, e1 = route_ref[0:1, :], route_ref[1:2, :]
     rank = rank_in_group(e0 // members, groups)
     row = lax.broadcasted_iota(jnp.int32, (groups * members * slots, rows), 0)
-    expert = row // slots
+    block = row // (slots * members)
+    group = block % (groups // cores) * cores + block // (groups // cores)
+    expert = group * members + row // slots % members
     weight = jnp.where(expert == e0, gw_ref[0:1, :], 0.0) + jnp.where(expert == e1, gw_ref[1:2, :], 0.0)
     weight = jnp.where(row % slots == rank, weight, 0.0).T
     high = weight.astype(BF)
     return jnp.concatenate([high, (weight - high.astype(F32)).astype(BF)], axis=0)
 
 
-def expert_kernel(groups, members, x_ref, wg_ref, wu_ref, wd_ref, route_ref, gw_ref, out_ref, pick_ref):
-    pick_ref[...] = selection(groups, members, x_ref.shape[1], route_ref, gw_ref)
+def expert_kernel(groups, members, cores, x_ref, wg_ref, wu_ref, wd_ref, route_ref, gw_ref, out_ref, pick_ref):
+    pick_ref[...] = selection(groups, members, cores, x_ref.shape[1], route_ref, gw_ref)
     blocks, slots, width = x_ref.shape
     step = blocks // 2
     half = wg_ref.shape[1] // 2
@@ -89,7 +94,8 @@
 
 def local(tokens, norm_gain, w_gate, w_up, w_down, routing, gate_weight):
     rows, width = tokens.shape
-    groups = lax.axis_size("ep")
+    cores = lax.axis_size("core")
+    groups = lax.axis_size("chip") * cores
     members = lax.axis_size("tp")
     experts = groups * members
     slots = rows // groups
@@ -105,7 +111,7 @@
         name="lead",
     )()
     pick = pl.pallas_call(
-        lambda *refs: slots_kernel(groups, members, *refs),
+        lambda *refs: slots_kernel(groups, members, cores, *refs),
         out_shape=jax.ShapeDtypeStruct((rows, rows), BF),
         compiler_params=params,
         name="slots",
@@ -116,10 +122,10 @@
         compiler_params=params,
         name="dispatch",
     )(pick, tokens, norm_gain.reshape(1, width))
-    arrived = lax.all_to_all(outgoing.reshape(experts, slots, width), AXES, split_axis=0, concat_axis=0, tiled=True)
+    arrived = lax.all_to_all(outgoing.reshape(experts, slots, width), ORDER, split_axis=0, concat_axis=0, tiled=True)
     in_vmem = pl.BlockSpec(memory_space=pltpu.VMEM)
     answered, weighted = pl.pallas_call(
-        lambda *refs: expert_kernel(groups, members, *refs),
+        lambda *refs: expert_kernel(groups, members, cores, *refs),
         in_specs=[in_vmem] * 6,
         out_specs=[in_vmem] * 2,
         out_shape=[
@@ -129,7 +135,7 @@
         compiler_params=params,
         name="expert",
     )(arrived, w_gate[0], w_up[0], w_down[0], route, weights)
-    returned = lax.all_to_all(answered, AXES, split_axis=0, concat_axis=0, tiled=True)
+    returned = lax.all_to_all(answered, ORDER, split_axis=0, concat_axis=0, tiled=True)
     return pl.pallas_call(
         combine_kernel,
         in_specs=[in_vmem] * 2,
@@ -142,6 +148,8 @@
 
 
 def solution(mesh):
+    shape = (mesh.shape["ep"] // CORES, CORES, mesh.shape["tp"])
+    mesh = Mesh(mesh.devices.reshape(shape), AXES)
     placed = (
         P(AXES, None),
         P(),

time: 82.9 us -> 81.1 us (0.978)
  blocking collectives: 76.2 us -> 74.4 us
    all_to_all x2, blocking collectives: 76.2 us -> 74.4 us  [the longest x1 40 us: local(): lax.all_to_all(outgoing.reshape(experts, slots, width), ORDER, split_axis...]
where the time goes in v7:
time: 81.1 us; the launch traced here: 81 us
  blocking collectives  74.4 us (92%)
  Pallas kernels  5.58 us (7%)
  local copies, waits for them, and re-layouts  0.91 us (1%)
    all_to_all x1, blocking collectives, local(): lax.all_to_all(outgoing.reshape(experts, slots, width), ORDER, split_axis...  40 us
    all_to_all x1, blocking collectives, local(): lax.all_to_all(answered, ORDER, split_axis=0, concat_axis=0, tiled=True)  34.5 us
    pallas_call x1, Pallas kernels, local(): pl.pallas_call(lambda *refs: expert_kernel(groups, members, cores, *refs)...  3.52 us

profile of v7, /device:TPU:1, one launch (start us, length us, event | category | flops | bytes accessed | tf_op | source)
XLA Modules:
  0.0 81.0 jit_solution(2874947519560804996)
XLA Ops:
  0.0 0.0 copy-start.5
  0.0 0.0 copy-start.4
  0.0 0.0 copy-start.3
  0.0 0.7 copy-done.5
  0.7 0.2 slots.1.refs_0_
  0.8 0.0 copy-done.4
  0.8 0.2 copy-done.3
  1.1 0.0 copy-start.2
  1.1 0.5 dispatch.1
  1.6 0.0 copy-start
  1.6 0.0 copy-start.1
  1.6 0.0 copy-start.6
  1.6 40.0 %all_to_all.10.refs_0_ = bf16[128,4,2048]{2,1,0:T(4,128)(2,1)S(1)} all-to-all(bf16[128,4,2048]{2,1,0:T(4,128)(2,1)S(1)} %bitcast.7), channel_id=1, replica_groups=mesh['chip'=16,'core'=2,'tp'=4] {'core','chip','tp'}, dimensions={0} | all-to-all | bytes 4194304 | tf_op jit(solution)/shard_map/all_to_all | solution.py:125
  41.6 0.0 copy-done.2
  41.6 0.0 copy-done
  41.6 0.0 copy-done.1
  41.6 0.0 copy-done.6
  41.6 3.5 %expert.1 = (bf16[128,4,2048]{2,1,0:T(4,128)(2,1)S(1)}, bf16[256,512]{1,0:T(8,128)(2,1)S(1)}) custom-call(bf16[128,4,2048]{2,1,0:T(4,128)(2,1)S(1)} %all_to_all.10.refs_0_, bf16[2048,512]{1,0:T(8,128)(2,1)S(1)} %bitcast.8, bf16[2048,512]{1,0:T(8,128)(2,1)S(1)} %bitcast.9, bf16[512,2048]{1,0:T(8,128)(2,1)S(1)} %bitcast.10, s32[2,128]{1,0:T(2,128)S(1)} %bitcast.13, ...), custom_call_target="tpu_custom_call" | custom-call | tf_op jit(solution)/shard_map/expert/pallas_call | solution.py:127
  45.1 34.5 %all_to_all.11.r_ref = bf16[128,4,2048]{2,1,0:T(4,128)(2,1)S(1)} all-to-all(bf16[128,4,2048]{2,1,0:T(4,128)(2,1)S(1)} %get-tuple-element.7), channel_id=1, replica_groups=mesh['chip'=16,'core'=2,'tp'=4] {'core','chip','tp'}, dimensions={0} | all-to-all | bytes 4194304 | tf_op jit(solution)/shard_map/all_to_all | solution.py:138
  79.6 1.4 %combine.1 = bf16[128,2048]{1,0:T(8,128)(2,1)} custom-call(bf16[128,4,2048]{2,1,0:T(4,128)(2,1)S(1)} %all_to_all.11.r_ref, bf16[256,512]{1,0:T(8,128)(2,1)S(1)} %get-tuple-element.8.pick_ref), custom_call_target="tpu_custom_call" | custom-call | tf_op jit(solution)/shard_map/combine/pallas_call | solution.py:139
  (1 shorter events, 0.0 us)
Async XLA Ops:
  0.0 0.7 copy-start.5
  0.0 0.8 %copy-start.4 = (f32[2048]{0:T(1024)S(1)}, f32[2048]{0:T(1024)}, u32[]{:S(2)}) copy-start(f32[2048]{0:T(1024)} %param.8) | copy-start | bytes 24580
  0.0 1.1 %copy-start.3 = (bf16[128,2048]{1,0:T(8,128)(2,1)S(1)}, bf16[128,2048]{1,0:T(8,128)(2,1)}, u32[]{:S(2)}) copy-start(bf16[128,2048]{1,0:T(8,128)(2,1)} %refs_1_.1) | copy-start | bytes 1572868
  1.1 40.5 %copy-start.2 = (bf16[1,512,2048]{2,1,0:T(8,128)(2,1)S(1)}, bf16[1,512,2048]{2,1,0:T(8,128)(2,1)}, u32[]{:S(2)}) copy-start(bf16[1,512,2048]{2,1,0:T(8,128)(2,1)} %param.11) | copy-start | bytes 6291460
  1.6 40.0 %copy-start = (bf16[1,2048,512]{2,1,0:T(8,128)(2,1)S(1)}, bf16[1,2048,512]{2,1,0:T(8,128)(2,1)}, u32[]{:S(2)}) copy-start(bf16[1,2048,512]{2,1,0:T(8,128)(2,1)} %param.9) | copy-start | bytes 6291460
  1.6 40.0 %copy-start.1 = (bf16[1,2048,512]{2,1,0:T(8,128)(2,1)S(1)}, bf16[1,2048,512]{2,1,0:T(8,128)(2,1)}, u32[]{:S(2)}) copy-start(bf16[1,2048,512]{2,1,0:T(8,128)(2,1)} %param.10) | copy-start | bytes 6291460
  1.6 40.0 %copy-start.6 = (f32[128,2]{0,1:T(2,128)S(1)}, f32[128,2]{0,1:T(2,128)}, u32[]{:S(2)}) copy-start(f32[128,2]{0,1:T(2,128)} %param.13) | copy-start | bytes 3076

commit v8 on v7

--- a/solution.py
+++ b/solution.py
@@ -77,15 +77,14 @@
 def combine_kernel(r_ref, pick_ref, out_hbm, out_ref, sems):
     blocks, slots, width = r_ref.shape
     rows = out_ref.shape[0]
-    parts = sems.shape[0]
-    step = width // parts
     pick = pick_ref[...]
     copies = []
-    for p in range(parts):
-        span = pl.ds(p * step, step)
-        r = r_ref[:, :, p * step:(p + 1) * step].reshape(blocks * slots, step)
+    cut = width * 3 // 4
+    for p, (at, step) in enumerate(((0, cut), (cut, width - cut))):
+        span = pl.ds(at, step)
+        r = r_ref[:, :, at:at + step].reshape(blocks * slots, step)
         out = jnp.dot(pick, r, preferred_element_type=F32)
-        out_ref[:, p * step:(p + 1) * step] = (out[:rows] + out[rows:]).astype(BF)
+        out_ref[:, at:at + step] = (out[:rows] + out[rows:]).astype(BF)
         copies.append(pltpu.make_async_copy(out_ref.at[:, span], out_hbm.at[:, span], sems.at[p]))
         copies[-1].start()
     for copy in copies:
@@ -141,7 +140,7 @@
         in_specs=[in_vmem] * 2,
         out_specs=pl.BlockSpec(memory_space=pltpu.HBM),
         out_shape=jax.ShapeDtypeStruct((rows, width), BF),
-        scratch_shapes=[pltpu.VMEM((rows, width), BF), pltpu.SemaphoreType.DMA((4,))],
+        scratch_shapes=[pltpu.VMEM((rows, width), BF), pltpu.SemaphoreType.DMA((2,))],
         compiler_params=params,
         name="combine",
     )(returned, weighted)

time: 81.1 us -> 81.1 us (level)
  no operation moved by 1% of the time
where the time goes in v8:
time: 81.1 us; the launch traced here: 81 us
  blocking collectives  74.4 us (92%)
  Pallas kernels  5.56 us (7%)
  local copies, waits for them, and re-layouts  0.91 us (1%)
    all_to_all x1, blocking collectives, local(): lax.all_to_all(outgoing.reshape(experts, slots, width), ORDER, split_axis...  40 us
    all_to_all x1, blocking collectives, local(): lax.all_to_all(answered, ORDER, split_axis=0, concat_axis=0, tiled=True)  34.5 us
    pallas_call x1, Pallas kernels, local(): pl.pallas_call(lambda *refs: expert_kernel(groups, members, cores, *refs)...  3.52 us

profile of v8, /device:TPU:1, one launch (start us, length us, event | category | flops | bytes accessed | tf_op | source)
XLA Modules:
  0.0 81.0 jit_solution(7486645228207035534)
XLA Ops:
  0.0 0.0 copy-start.5
  0.0 0.0 copy-start.4
  0.0 0.0 copy-start.3
  0.0 0.7 copy-done.5
  0.7 0.2 slots.1.refs_0_
  0.8 0.0 copy-done.4
  0.8 0.2 copy-done.3
  1.1 0.0 copy-start.2
  1.1 0.5 dispatch.1
  1.6 0.0 copy-start
  1.6 0.0 copy-start.1
  1.6 0.0 copy-start.6
  1.6 40.0 %all_to_all.10.refs_0_ = bf16[128,4,2048]{2,1,0:T(4,128)(2,1)S(1)} all-to-all(bf16[128,4,2048]{2,1,0:T(4,128)(2,1)S(1)} %bitcast.7), channel_id=1, replica_groups=mesh['chip'=16,'core'=2,'tp'=4] {'core','chip','tp'}, dimensions={0} | all-to-all | bytes 4194304 | tf_op jit(solution)/shard_map/all_to_all | solution.py:124
  41.6 0.0 copy-done.2
  41.6 0.0 copy-done
  41.6 0.0 copy-done.1
  41.6 0.0 copy-done.6
  41.6 3.5 %expert.1 = (bf16[128,4,2048]{2,1,0:T(4,128)(2,1)S(1)}, bf16[256,512]{1,0:T(8,128)(2,1)S(1)}) custom-call(bf16[128,4,2048]{2,1,0:T(4,128)(2,1)S(1)} %all_to_all.10.refs_0_, bf16[2048,512]{1,0:T(8,128)(2,1)S(1)} %bitcast.8, bf16[2048,512]{1,0:T(8,128)(2,1)S(1)} %bitcast.9, bf16[512,2048]{1,0:T(8,128)(2,1)S(1)} %bitcast.10, s32[2,128]{1,0:T(2,128)S(1)} %bitcast.13, ...), custom_call_target="tpu_custom_call" | custom-call | tf_op jit(solution)/shard_map/expert/pallas_call | solution.py:126
  45.1 34.5 %all_to_all.11.r_ref = bf16[128,4,2048]{2,1,0:T(4,128)(2,1)S(1)} all-to-all(bf16[128,4,2048]{2,1,0:T(4,128)(2,1)S(1)} %get-tuple-element.7), channel_id=1, replica_groups=mesh['chip'=16,'core'=2,'tp'=4] {'core','chip','tp'}, dimensions={0} | all-to-all | bytes 4194304 | tf_op jit(solution)/shard_map/all_to_all | solution.py:137
  79.6 1.4 %combine.1 = bf16[128,2048]{1,0:T(8,128)(2,1)} custom-call(bf16[128,4,2048]{2,1,0:T(4,128)(2,1)S(1)} %all_to_all.11.r_ref, bf16[256,512]{1,0:T(8,128)(2,1)S(1)} %get-tuple-element.8.pick_ref), custom_call_target="tpu_custom_call" | custom-call | tf_op jit(solution)/shard_map/combine/pallas_call | solution.py:138
  (1 shorter events, 0.0 us)
Async XLA Ops:
  0.0 0.7 copy-start.5
  0.0 0.8 %copy-start.4 = (f32[2048]{0:T(1024)S(1)}, f32[2048]{0:T(1024)}, u32[]{:S(2)}) copy-start(f32[2048]{0:T(1024)} %param.8) | copy-start | bytes 24580
  0.0 1.1 %copy-start.3 = (bf16[128,2048]{1,0:T(8,128)(2,1)S(1)}, bf16[128,2048]{1,0:T(8,128)(2,1)}, u32[]{:S(2)}) copy-start(bf16[128,2048]{1,0:T(8,128)(2,1)} %refs_1_.1) | copy-start | bytes 1572868
  1.1 40.5 %copy-start.2 = (bf16[1,512,2048]{2,1,0:T(8,128)(2,1)S(1)}, bf16[1,512,2048]{2,1,0:T(8,128)(2,1)}, u32[]{:S(2)}) copy-start(bf16[1,512,2048]{2,1,0:T(8,128)(2,1)} %param.11) | copy-start | bytes 6291460
  1.6 40.0 %copy-start = (bf16[1,2048,512]{2,1,0:T(8,128)(2,1)S(1)}, bf16[1,2048,512]{2,1,0:T(8,128)(2,1)}, u32[]{:S(2)}) copy-start(bf16[1,2048,512]{2,1,0:T(8,128)(2,1)} %param.9) | copy-start | bytes 6291460
  1.6 40.0 %copy-start.1 = (bf16[1,2048,512]{2,1,0:T(8,128)(2,1)S(1)}, bf16[1,2048,512]{2,1,0:T(8,128)(2,1)}, u32[]{:S(2)}) copy-start(bf16[1,2048,512]{2,1,0:T(8,128)(2,1)} %param.10) | copy-start | bytes 6291460
  1.6 40.0 %copy-start.6 = (f32[128,2]{0,1:T(2,128)S(1)}, f32[128,2]{0,1:T(2,128)}, u32[]{:S(2)}) copy-start(f32[128,2]{0,1:T(2,128)} %param.13) | copy-start | bytes 3076
